TPU v7x, 32 devices: a whole 2x2x4 slice. The times are simulated.
32 devices in a mesh: kv: 8 (over z, y), tp: 4 (over x, core).
Axes of the slice: x: 2, y: 2, z: 4, core: 2. Of those that a mesh axis runs over, the one named last changes fastest.
Arguments:
- hidden_vectors: bfloat16 [64, 2048], P(None, 'kv'), may hold values from -24 to 24
- input_norm_gain: float32 [2048], P('kv'), may hold values from 0.1 to 1.9
- gate_matrix: bfloat16 [2048, 4096], P('kv', 'tp'), may hold values from -0.125 to 0.125
- value_matrix: bfloat16 [2048, 4096], P('kv', 'tp'), may hold values from -0.125 to 0.125
- write_matrix: bfloat16 [2048, 2048], P('kv', 'tp'), may hold values from -0.125 to 0.125
- read_matrix: bfloat16 [2048, 2048], P('kv', 'tp'), may hold values from -0.125 to 0.125
- step_matrix: bfloat16 [2048, 64], P('kv', 'tp'), may hold values from -0.125 to 0.125
- raw_value_rows: bfloat16 [16, 7, 4096], P('kv', None, 'tp'), may hold values from -6 to 6
- raw_write_rows: bfloat16 [16, 7, 2048], P('kv', None, 'tp'), may hold values from -6 to 6
- raw_read_rows: bfloat16 [16, 7, 2048], P('kv', None, 'tp'), may hold values from -6 to 6
- value_filter_taps: bfloat16 [4, 4096], P(None, 'tp'), may hold values from -3 to 3
- write_filter_taps: bfloat16 [4, 2048], P(None, 'tp'), may hold values from -3 to 3
- read_filter_taps: bfloat16 [4, 2048], P(None, 'tp'), may hold values from -3 to 3
- step_size_bias: float32 [64], P('tp'), may hold values from -3 to 0
- rate_logarithm: float32 [64], P('tp'), may hold values from -4 to 0.5
- direct_path_gain: float32 [64], P('tp'), may hold values from 0.1 to 1.9
- prior_step_preact: float32 [16, 4, 64], P('kv', None, 'tp'), may hold values from -6 to 6
- extra_log_decay: float32 [16, 8, 64], P('kv', None, 'tp'), may hold values from -0.7 to 0, as said below
- accepted: int32 [16], P('kv'), may hold values from 0 to 4
- prior_state: float32 [16, 64, 64, 128], P('kv', 'tp'), may hold values from -6 to 6
- group_norm_gain: float32 [4096], P('tp'), may hold values from 0.1 to 1.9
- output_matrix: bfloat16 [4096, 2048], P('tp', 'kv'), may hold values from -0.09375 to 0.09375
Outputs:
- mixer_out: bfloat16 [64, 2048], P('tp', 'kv')
- resumed_state: float32 [16, 64, 64, 128], P('kv', 'tp')
Inputs may be any that keep to these rules, and one draw needn't show every extreme that they name: `extra_log_decay`: zero at most positions.
All inputs are finite; a program needn't handle non-finite values.
Results may differ from a plain program's by a relative error of at most 0.0095.
Values may be sent and summed in bfloat16 or wider, within the bound.
A program may use at most 64 MiB of HBM per device.

v0:
```python
import jax
import jax.numpy as jnp
from jax import lax
from jax.sharding import PartitionSpec as P

D = 2048
HEAD_DIM = 64
GROUPS = 16
STATE = 128
TAPS = 4
DRAFT_TOKENS = 4
INNER = 4096


epsilon = 1e-06
highest = lax.Precision.HIGHEST


def conv_rows(row_block, taps):
    length_rows = row_block.shape[1] - (TAPS - 1)
    result = jnp.zeros((row_block.shape[0], length_rows, row_block.shape[2]), jnp.float32)
    for tap_index in range(TAPS):
        result = result + row_block[:, tap_index : tap_index + length_rows].astype(
            jnp.float32
        ) * taps[tap_index].astype(jnp.float32)
    return jax.nn.silu(result)


def resume_state(start_state, values, writes, head_step_size, decay_logarithm, accepted):
    live_mask = (jnp.arange(values.shape[1])[None, :] < accepted[:, None]).astype(jnp.float32)
    kept_decay = decay_logarithm * live_mask[:, :, None]
    total_decay = jnp.sum(kept_decay, axis=1)
    tail_decay = total_decay[:, None, :] - jnp.cumsum(kept_decay, axis=1)
    coefficient = live_mask[:, :, None] * jnp.exp(tail_decay) * head_step_size
    added = jnp.einsum("skh,skhp,skhn->shpn", coefficient, values, writes, precision=highest)
    return jnp.exp(total_decay)[:, :, None, None] * start_state + added


def dual_block(
    values, writes, reads, head_step_size, decay_logarithm, direct_path_gain, start_state
):
    cumulative = jnp.cumsum(decay_logarithm, axis=1)
    carried = jnp.exp(cumulative)[..., None] * jnp.einsum(
        "skhn,shpn->skhp", reads, start_state, precision=highest
    )
    order = jnp.arange(cumulative.shape[1])
    causal = order[:, None] >= order[None, :]
    difference = cumulative[:, :, None, :] - cumulative[:, None, :, :]
    decay_weight = jnp.where(causal[None, :, :, None], jnp.exp(jnp.minimum(difference, 0.0)), 0.0)
    inner_terms = jnp.einsum("sthn,suhn->stuh", reads, writes, precision=highest)
    within = jnp.einsum(
        "stuh,suh,suhp->sthp", inner_terms * decay_weight, head_step_size, values, precision=highest
    )
    return carried + within + direct_path_gain[None, None, :, None] * values


def mixer_kernel_body(
    output_gate,
    fresh_values,
    fresh_writes,
    fresh_reads,
    step_preact,
    raw_value_rows,
    raw_write_rows,
    raw_read_rows,
    value_filter_taps,
    write_filter_taps,
    read_filter_taps,
    step_size_bias,
    rate_logarithm,
    direct_path_gain,
    prior_step_preact,
    extra_log_decay,
    accepted,
    prior_state,
    group_norm_gain,
):
    seq_count = raw_value_rows.shape[0]
    head_count = step_preact.shape[2]
    group_count = fresh_writes.shape[2] // STATE
    per_group = head_count // group_count
    window = accepted[:, None] + jnp.arange(TAPS - 1, dtype=jnp.int32)[None, :]

    def current(row_block, new_rows, taps):
        earlier = jnp.take_along_axis(row_block, window[:, :, None], axis=1)
        return conv_rows(jnp.concatenate([earlier, new_rows], axis=1), taps)

    conv_values = current(raw_value_rows, fresh_values, value_filter_taps).reshape(
        seq_count, DRAFT_TOKENS, head_count, HEAD_DIM
    )
    conv_writes = current(raw_write_rows, fresh_writes, write_filter_taps).reshape(
        seq_count, DRAFT_TOKENS, group_count, STATE
    )
    conv_reads = current(raw_read_rows, fresh_reads, read_filter_taps).reshape(
        seq_count, DRAFT_TOKENS, group_count, STATE
    )
    last_values = conv_rows(raw_value_rows, value_filter_taps).reshape(
        seq_count, DRAFT_TOKENS, head_count, HEAD_DIM
    )
    last_writes = conv_rows(raw_write_rows, write_filter_taps).reshape(
        seq_count, DRAFT_TOKENS, group_count, STATE
    )
    head_decay_rate = jnp.exp(rate_logarithm)
    head_step_size = jax.nn.softplus(step_preact + step_size_bias)
    decay_logarithm = -head_decay_rate * head_step_size + extra_log_decay[:, DRAFT_TOKENS:]
    prior_step = jax.nn.softplus(prior_step_preact + step_size_bias)
    prior_decay = -head_decay_rate * prior_step + extra_log_decay[:, :DRAFT_TOKENS]
    restored_state = resume_state(
        prior_state,
        last_values,
        jnp.repeat(last_writes, per_group, axis=2),
        prior_step,
        prior_decay,
        accepted,
    )
    mixed_heads = dual_block(
        conv_values,
        jnp.repeat(conv_writes, per_group, axis=2),
        jnp.repeat(conv_reads, per_group, axis=2),
        head_step_size,
        decay_logarithm,
        direct_path_gain,
        restored_state,
    )
    gated = mixed_heads.reshape(seq_count, DRAFT_TOKENS, -1) * jax.nn.silu(
        output_gate.astype(jnp.float32)
    )
    group_width = INNER // GROUPS
    grouped = gated.reshape(seq_count, DRAFT_TOKENS, -1, group_width)
    scale = lax.rsqrt(jnp.mean(grouped * grouped, axis=-1, keepdims=True) + epsilon)
    normalized_hidden = (grouped * scale).reshape(seq_count, DRAFT_TOKENS, -1) * group_norm_gain
    return (
        normalized_hidden.astype(jnp.bfloat16).reshape(seq_count * DRAFT_TOKENS, -1),
        restored_state,
    )


def per_device(
    hidden_vectors,
    input_norm_gain,
    gate_matrix,
    value_matrix,
    write_matrix,
    read_matrix,
    step_matrix,
    raw_value_rows,
    raw_write_rows,
    raw_read_rows,
    value_filter_taps,
    write_filter_taps,
    read_filter_taps,
    step_size_bias,
    rate_logarithm,
    direct_path_gain,
    prior_step_preact,
    extra_log_decay,
    accepted,
    prior_state,
    group_norm_gain,
    output_matrix,
):
    floats_in = hidden_vectors.astype(jnp.float32)
    square_part = jnp.sum(floats_in * floats_in, axis=1)
    scaled = (floats_in * input_norm_gain).astype(jnp.bfloat16)
    seq_count = raw_value_rows.shape[0]
    role_weights = (gate_matrix, value_matrix, write_matrix, read_matrix)
    widths = tuple((weight.shape[1] for weight in role_weights))
    joined = jnp.concatenate(role_weights, axis=1)
    main_part = jnp.dot(scaled, joined, preferred_element_type=jnp.float32)
    step_part = jnp.dot(scaled, step_matrix, preferred_element_type=jnp.float32)
    main_sum, step_sum, own_squares = (
        lax.psum_scatter(main_part, "kv", scatter_dimension=0, tiled=True),
        lax.psum_scatter(step_part, "kv", scatter_dimension=0, tiled=True),
        lax.psum_scatter(square_part, "kv", scatter_dimension=0, tiled=True),
    )
    inverse = lax.rsqrt(own_squares / D + epsilon)[:, None]
    projected = (inverse * main_sum).astype(jnp.bfloat16).reshape(seq_count, DRAFT_TOKENS, -1)
    first_cut = widths[0]
    second_cut = first_cut + widths[1]
    third_cut = second_cut + widths[2]
    output_gate = projected[:, :, :first_cut]
    fresh_values = projected[:, :, first_cut:second_cut]
    fresh_writes = projected[:, :, second_cut:third_cut]
    fresh_reads = projected[:, :, third_cut:]
    step_preact = (inverse * step_sum).reshape(seq_count, DRAFT_TOKENS, -1)
    normalized_hidden, restored_state = mixer_kernel_body(
        output_gate,
        fresh_values,
        fresh_writes,
        fresh_reads,
        step_preact,
        raw_value_rows,
        raw_write_rows,
        raw_read_rows,
        value_filter_taps,
        write_filter_taps,
        read_filter_taps,
        step_size_bias,
        rate_logarithm,
        direct_path_gain,
        prior_step_preact,
        extra_log_decay,
        accepted,
        prior_state,
        group_norm_gain,
    )
    partial_value = jnp.dot(
        lax.all_gather(normalized_hidden, "kv", axis=0, tiled=True),
        output_matrix,
        preferred_element_type=jnp.float32,
    )
    mixer_out = lax.psum_scatter(
        partial_value.astype(jnp.bfloat16), "tp", scatter_dimension=0, tiled=True
    )
    return (mixer_out, restored_state)


def solution(mesh):
    placed = (
        P(None, "kv"),
        P("kv"),
        P("kv", "tp"),
        P("kv", "tp"),
        P("kv", "tp"),
        P("kv", "tp"),
        P("kv", "tp"),
        P("kv", None, "tp"),
        P("kv", None, "tp"),
        P("kv", None, "tp"),
        P(None, "tp"),
        P(None, "tp"),
        P(None, "tp"),
        P("tp"),
        P("tp"),
        P("tp"),
        P("kv", None, "tp"),
        P("kv", None, "tp"),
        P("kv"),
        P("kv", "tp", None, None),
        P("tp"),
        P("tp", "kv"),
    )
    return jax.shard_map(
        per_device,
        mesh=mesh,
        in_specs=placed,
        out_specs=(P("tp", "kv"), P("kv", "tp", None, None)),
        check_vma=False,
    )
```

profile of v0, /device:TPU:0, one launch (start us, length us, event | category | flops | bytes accessed | tf_op | source)
XLA Modules:
  0.0 141.4 jit_solution(11478069576930128547)
XLA Ops:
  7.2 0.0 copy-start
  7.2 0.0 copy-start.19
  7.2 0.0 copy-start.6
  7.2 0.0 copy-start.15
  7.2 0.0 copy-start.18
  7.2 0.0 copy-start.11
  7.2 0.0 copy-start.17
  7.2 0.0 copy-start.14
  7.3 0.0 reduce-scatter.3.cloned.1.call-start
  7.3 2.7 %fusion = f32[64,3072]{1,0:T(8,128)} fusion(bf16[256,512]{1,0:T(8,128)(2,1)} %param.29, bf16[256,512]{1,0:T(8,128)(2,1)} %param.28, bf16[256,1024]{1,0:T(8,128)(2,1)} %param.27, bf16[256,1024]{1,0:T(8,128)(2,1)} %param.26, bf16[64,256]{1,0:T(8,128)(2,1)} %param.24, f32[256]{0:T(256)} %param.25), kind=kOutput, calls=%fused_computation.3 | convolution fusion | flops 107003904 | bytes 2393088 | tf_op jit(solution)/shard_map/dot_general | solution.py:169
  10.0 0.0 copy-start.2
  10.1 0.0 copy-start.9
  10.1 0.0 copy-start.7
  10.1 0.0 reduce-scatter.3.cloned.1.call-update
  10.1 0.0 copy-start.3
  10.1 0.0 reduce-scatter.5.cloned.1.call-start
  10.2 0.1 fusion.9
  10.3 0.0 copy-done.18
  10.3 0.1 shift-left_or_fusion
  10.4 0.1 and_bitcast_fusion
  10.5 0.1 compare_convert_fusion
  10.5 0.0 copy-done.15
  10.5 0.1 fusion.19
  10.7 0.0 copy-done.17
  10.7 39.3 %all-reduce.2 = (f32[64]{0:T(128)S(1)}, f32[64,16]{1,0:T(8,128)S(1)}) all-reduce(f32[64]{0:T(128)S(1)} %fusion.9, f32[64,16]{1,0:T(8,128)S(1)} %fusion.19), channel_id=2, replica_groups=mesh['kv'=8,'tp'=4] {'kv'}, use_global_device_ids=true, to_apply=%region_1.0.clone | all-reduce | flops 1088 | bytes 8704
  50.0 0.6 dynamic-slice
  51.3 0.1 fusion.31
  51.3 0.1 dynamic-slice_multiply_fusion
  51.4 0.0 copy-done.14
  51.4 0.0 copy-done.12
  51.4 0.1 fusion.34
  51.5 0.1 copy.94
  51.6 0.1 reshape.309
  51.7 0.6 gather_fusion.1
  52.4 0.6 gather_fusion.2
  53.0 0.6 gather_fusion
  53.7 0.1 multiply_multiply_fusion
  53.8 0.1 copy.80
  53.9 0.1 compare_and_fusion
  54.0 0.1 broadcast_select_fusion
  54.1 0.1 broadcast_select_fusion.2
  54.3 23.7 %reduce-scatter.3.cloned.1.call-done = f32[8,3072]{1,0:T(8,128)} async-done(((f32[64,3072]{1,0:T(8,128)}), f32[8,3072]{1,0:T(8,128)}) %reduce-scatter.3.cloned.1.call-update) | async-done | bytes 98320 | tf_op jit(solution)/shard_map/reduce_scatter | solution.py:172
  78.0 1.0 multiply_convert_fusion
  79.0 0.1 divide_multiply_fusion.1
  79.1 0.1 reshape.268
  79.2 0.1 reshape.274
  79.3 0.1 fusion.25
  79.4 1.9 %convolution_add_fusion = f32[2,16,64,128]{3,2,1,0:T(8,128)S(1)} fusion(f32[2,4,16,128]{3,1,2,0:T(4,128)S(1)} %bitcast.53, f32[2,16,64,128]{3,2,1,0:T(8,128)S(1)} %copy-done.3, f32[2,16]{1,0:T(2,128)S(1)} %exp.54, f32[2,4,16,64]{3,2,1,0:T(8,128)S(1)} %reshape.268, f32[2,4,16]{1,2,0:T(8,128)S(1)} %copy.80), kind=kOutput, calls=%fused_computation.11 | convolution fusion | flops 13115392 | bytes 2196096 | tf_op jit(solution)/shard_map/skh,skhp,skhn->shpn/dot_general | solution.py:35
  81.4 0.0 copy-start.1
  81.4 0.0 copy-start.16
  81.5 0.0 copy-start.13
  81.5 1.7 %fusion.38 = f32[2,16,64,4]{2,3,1,0:T(4,128)S(1)} fusion(f32[2,16,64,128]{3,2,1,0:T(8,128)S(1)} %convolution_add_fusion, f32[2,4,16,128]{3,1,2,0:T(4,128)S(1)} %bitcast.51), kind=kOutput, calls=%fused_computation.103 | convolution fusion | flops 12582912 | bytes 1146880 | tf_op jit(solution)/shard_map/skhn,shpn->skhp/dot_general | solution.py:43
  83.2 0.1 broadcast_multiply_fusion
  83.3 0.4 fusion.8
  83.7 0.4 fusion.12
  84.1 0.0 copy-done.16
  84.1 0.1 fusion.11
  84.2 0.1 reshape.277
  84.4 0.1 reduce_sum.29
  84.5 0.1 mul.339
  84.7 30.5 %all_gather.3 = bf16[64,1024]{1,0:T(8,128)(2,1)S(1)} all-gather(bf16[8,1024]{1,0:T(8,128)(2,1)S(1)} %reshape.278), channel_id=1, replica_groups=mesh['kv'=8,'tp'=4] {'kv'}, dimensions={0}, use_global_device_ids=true | all-gather | bytes 147456 | tf_op jit(solution)/shard_map/all_gather | solution.py:208
  115.2 0.8 convolution_convert_fusion
  116.0 0.0 reduce-scatter.5.cloned.1.call-update
  116.1 18.5 %reduce-scatter.5.cloned.1.call-done = bf16[16,256]{1,0:T(8,128)(2,1)} async-done(((bf16[64,256]{1,0:T(8,128)(2,1)}), bf16[16,256]{1,0:T(8,128)(2,1)}) %reduce-scatter.5.cloned.1.call-update) | async-done | bytes 8208 | tf_op jit(solution)/shard_map/reduce_scatter | solution.py:212
  (46 shorter events, 0.6 us)
Async XLA Ops:
  7.2 108.0 %copy-start = (bf16[1024,256]{1,0:T(8,128)(2,1)S(1)}, bf16[1024,256]{1,0:T(8,128)(2,1)}, u32[]{:S(2)}) copy-start(bf16[1024,256]{1,0:T(8,128)(2,1)} %param.45) | copy-start | bytes 1572868
  7.2 42.8 %copy-start.19 = (u32[32]{0:T(128)S(1)}, u32[32]{0:T(128)}, u32[]{:S(2)}) copy-start(u32[32]{0:T(128)} %constant.107) | copy-start | bytes 388
  7.2 3.0 %copy-start.6 = (bf16[64,256]{1,0:T(8,128)(2,1)S(1)}, bf16[64,256]{1,0:T(8,128)(2,1)}, u32[]{:S(2)}) copy-start(bf16[64,256]{1,0:T(8,128)(2,1)} %param.24) | copy-start | bytes 98308
  7.2 3.3 %copy-start.15 = (f32[256]{0:T(256)S(1)}, f32[256]{0:T(256)}, u32[]{:S(2)}) copy-start(f32[256]{0:T(256)} %param.25) | copy-start | bytes 3076
  7.2 3.1 %copy-start.18 = (s32[2]{0:T(128)S(1)}, s32[2]{0:T(128)}, u32[]{:S(2)}) copy-start(s32[2]{0:T(128)} %param.42) | copy-start | bytes 28
  7.2 3.3 %copy-start.11 = (bf16[256,16]{0,1:T(8,128)(2,1)S(1)}, bf16[256,16]{0,1:T(8,128)(2,1)}, u32[]{:S(2)}) copy-start(bf16[256,16]{0,1:T(8,128)(2,1)} %param.30) | copy-start | bytes 24580
  7.2 3.4 %copy-start.17 = (f32[16]{0:T(128)S(1)}, f32[16]{0:T(128)}, u32[]{:S(2)}) copy-start(f32[16]{0:T(128)} %param.38) | copy-start | bytes 196
  7.2 44.2 %copy-start.14 = (f32[16]{0:T(128)S(1)}, f32[16]{0:T(128)}, u32[]{:S(2)}) copy-start(f32[16]{0:T(128)} %param.37) | copy-start | bytes 196
  7.3 44.2 %copy-start.10 = (f32[2,4,16]{2,1,0:T(4,128)S(1)}, f32[2,4,16]{2,1,0:T(4,128)}, u32[]{:S(2)}) copy-start(f32[2,4,16]{2,1,0:T(4,128)} %param.40) | copy-start | bytes 1540
  7.3 44.2 %copy-start.12 = (f32[2,8,16]{2,1,0:T(8,128)S(1)}, f32[2,8,16]{2,1,0:T(8,128)}, u32[]{:S(2)}) copy-start(f32[2,8,16]{2,1,0:T(8,128)} %param.41) | copy-start | bytes 3076
  7.3 70.7 %reduce-scatter.3.cloned.1.call-start = ((), (), s32[]{:S(2)}) async-start(), calls=%async_computation.2 | async-start | bytes 884736 | tf_op jit(solution)/shard_map/reduce_scatter | solution.py:172
  10.0 41.7 %copy-start.5 = (bf16[2,7,512]{2,0,1:T(2,128)(2,1)S(1)}, bf16[2,7,512]{2,0,1:T(2,128)(2,1)}, u32[]{:S(2)}) copy-start(bf16[2,7,512]{2,0,1:T(2,128)(2,1)} %param.33) | copy-start | bytes 43012
  10.0 42.3 %copy-start.4 = (bf16[2,7,512]{2,0,1:T(2,128)(2,1)S(1)}, bf16[2,7,512]{2,0,1:T(2,128)(2,1)}, u32[]{:S(2)}) copy-start(bf16[2,7,512]{2,0,1:T(2,128)(2,1)} %param.32) | copy-start | bytes 43012
  10.0 43.0 %copy-start.8 = (bf16[4,512]{1,0:T(4,128)(2,1)S(1)}, bf16[4,512]{1,0:T(4,128)(2,1)}, u32[]{:S(2)}) copy-start(bf16[4,512]{1,0:T(4,128)(2,1)} %param.35) | copy-start | bytes 12292
  10.0 43.0 %copy-start.2 = (bf16[2,7,1024]{2,0,1:T(2,128)(2,1)S(1)}, bf16[2,7,1024]{2,0,1:T(2,128)(2,1)}, u32[]{:S(2)}) copy-start(bf16[2,7,1024]{2,0,1:T(2,128)(2,1)} %param.31) | copy-start | bytes 86020
  10.1 43.9 %copy-start.9 = (bf16[4,512]{1,0:T(4,128)(2,1)S(1)}, bf16[4,512]{1,0:T(4,128)(2,1)}, u32[]{:S(2)}) copy-start(bf16[4,512]{1,0:T(4,128)(2,1)} %param.36) | copy-start | bytes 12292
  10.1 43.9 %copy-start.7 = (bf16[4,1024]{1,0:T(4,128)(2,1)S(1)}, bf16[4,1024]{1,0:T(4,128)(2,1)}, u32[]{:S(2)}) copy-start(bf16[4,1024]{1,0:T(4,128)(2,1)} %param.34) | copy-start | bytes 24580
  10.1 69.3 %copy-start.3 = (f32[2,16,64,128]{3,2,1,0:T(8,128)S(1)}, f32[2,16,64,128]{3,2,1,0:T(8,128)}, u32[]{:S(2)}) copy-start(f32[2,16,64,128]{3,2,1,0:T(8,128)} %param.43) | copy-start | bytes 3145732
  10.1 124.4 %reduce-scatter.5.cloned.1.call-start = ((), (), s32[]{:S(2)}) async-start(), calls=%async_computation.3 | async-start | bytes 40960 | tf_op jit(solution)/shard_map/reduce_scatter | solution.py:212
  81.4 2.9 %copy-start.1 = (f32[2,16,64,128]{3,2,1,0:T(8,128)}, f32[2,16,64,128]{3,2,1,0:T(8,128)S(1)}, u32[]{:S(2)}) copy-start(f32[2,16,64,128]{3,2,1,0:T(8,128)S(1)} %convolution_add_fusion) | copy-start | bytes 3145732
  81.4 2.7 %copy-start.16 = (f32[16]{0:T(128)S(1)}, f32[16]{0:T(128)}, u32[]{:S(2)}) copy-start(f32[16]{0:T(128)} %param.39) | copy-start | bytes 196
  81.5 3.2 %copy-start.13 = (f32[1024]{0:T(1024)S(1)}, f32[1024]{0:T(1024)}, u32[]{:S(2)}) copy-start(f32[1024]{0:T(1024)} %param.44) | copy-start | bytes 12292
Sparse Core Ops, SparseCore 0:
  12.0 65.9 reduce-scatter.2
  116.2 18.3 reduce-scatter.4
where the time goes:
time: 142 us; the launch traced here: 141 us
  blocking collectives  69.9 us (49%)
  waiting for transfers between devices  42.3 us (30%)
  between operations  15.1 us (11%)
  matrix products  8.08 us (6%)
  local copies, waits for them, and re-layouts  3.45 us (2%)
  other arithmetic  2.55 us (2%)
    unnamed x1, blocking collectives  39.3 us
    all_gather x1, blocking collectives, per_device(): lax.all_gather(normalized_hidden, 'kv', axis=0, tiled=True)  30.5 us
    reduce_scatter x1, waiting for transfers between devices, per_device(): lax.psum_scatter(main_part, 'kv', scatter_dimension=0, tiled=True)  23.7 us
    reduce_scatter x1, waiting for transfers between devices, per_device(): lax.psum_scatter(partial_value.astype(jnp.bfloat16), 'tp', scatter_dimens...  18.5 us
  transfers between devices with their start and end apart: 2, of which 2 were waited for; matrix products, arithmetic and copies ran while one was open for 3% of the time, Pallas kernels for 0%

commit v1 on v0

v1 whole, which is shorter than its diff:
```python
import functools

import jax
import jax.numpy as jnp
from jax import lax
from jax.experimental import pallas as pl
from jax.experimental.pallas import tpu as pltpu
from jax.sharding import PartitionSpec as P

HEAD_DIM = 64
STATE = 128
TAPS = 4
DRAFT = 4
EPS = 1e-06
F32 = jnp.float32
BF16 = jnp.bfloat16


def iota(shape, dim):
    return lax.broadcasted_iota(jnp.int32, shape, dim)


def silu(x):
    return x / (1.0 + jnp.exp(-x))


def softplus(x):
    return jnp.maximum(x, 0.0) + jnp.log1p(jnp.exp(-jnp.abs(x)))


def dot(a, b, dims=((1,), (0,)), precision=None):
    return lax.dot_general(
        a, b, (dims, ((), ())), preferred_element_type=F32, precision=precision
    )


def split(x):
    high = x.astype(BF16)
    return high, (x - high.astype(F32)).astype(BF16)


def body(nkv, ntp, *refs):
    (
        hid_h, gain_h, gate_h, value_h, write_h, read_h, step_h,
        rawv_h, raww_h, rawr_h, tapv_h, tapw_h, tapr_h,
        bias_h, rate_h, direct_h, prior_h, extra_h, acc_h, state_h, gng_h, outm_h,
        out_ref, res_ref,
        hid, gain, gate, value, write, read, step, rawv, raww, rawr,
        tapv, tapw, tapr, bias, rate, direct, prior, extra, acc, state, gng, outm,
        sbuf, rbuf, saux, raux, gbuf, pbuf, qbuf, s_hi, s_lo,
        load_sem, send_sem, recv_sem, gsend_sem, grecv_sem, psend_sem, precv_sem,
    ) = refs
    me = lax.axis_index("kv")
    my_tp = lax.axis_index("tp")
    rows = sbuf.shape[1]
    seqs = rawv.shape[0]
    tokens, depth = hid.shape
    heads = step.shape[1]
    cv, cw = value.shape[1], write.shape[1]
    groups = cw // STATE
    width = cv // groups
    per_group = heads // groups
    raw_len = rawv.shape[1]
    MESH = pl.DeviceIdType.MESH

    loads = {}
    order = (
        ("hid", hid_h, hid), ("gain", gain_h, gain), ("step", step_h, step),
        ("write", write_h, write), ("read", read_h, read), ("value", value_h, value),
        ("gate", gate_h, gate), ("acc", acc_h, acc), ("rawv", rawv_h, rawv),
        ("raww", raww_h, raww), ("rawr", rawr_h, rawr), ("tapv", tapv_h, tapv),
        ("tapw", tapw_h, tapw), ("tapr", tapr_h, tapr), ("bias", bias_h, bias),
        ("rate", rate_h, rate), ("direct", direct_h, direct), ("prior", prior_h, prior),
        ("extra", extra_h, extra), ("state", state_h, state), ("gng", gng_h, gng),
        ("outm", outm_h, outm),
    )
    for i, (name, src, dst) in enumerate(order):
        loads[name] = pltpu.make_async_copy(src, dst, load_sem.at[i])
        loads[name].start()

    barrier = pltpu.get_barrier_semaphore()
    for off in range(1, nkv):
        pl.semaphore_signal(
            barrier, inc=1, device_id={"kv": lax.rem(me + off, nkv)}, device_id_type=MESH
        )
    for off in range(1, ntp):
        pl.semaphore_signal(
            barrier, inc=1, device_id={"tp": lax.rem(my_tp + off, ntp)}, device_id_type=MESH
        )

    loads["hid"].wait()
    loads["gain"].wait()
    loads["step"].wait()
    floats = hid[...].astype(F32)
    squares = jnp.sum(floats * floats, axis=1, keepdims=True)
    scaled = (floats * gain[...]).astype(BF16)
    saux[:, :, :STATE] = jnp.broadcast_to(squares, (tokens, STATE)).reshape(nkv, rows, STATE)
    saux[:, :, STATE:] = jnp.zeros((nkv, rows, STATE), F32)
    saux[:, :, STATE : STATE + heads] = dot(scaled, step[...]).reshape(nkv, rows, heads)

    sends = []

    def exchange(buffer, target, start, size, part):
        for off in range(1, nkv):
            peer = lax.rem(me + off, nkv)
            if size is None:
                src, dst = buffer.at[peer], target.at[off - 1]
            else:
                src = buffer.at[peer, :, pl.ds(start, size)]
                dst = target.at[off - 1, :, pl.ds(start, size)]
            copy = pltpu.make_async_remote_copy(
                src_ref=src, dst_ref=dst,
                send_sem=send_sem.at[part, off - 1], recv_sem=recv_sem.at[part, off - 1],
                device_id={"kv": peer}, device_id_type=MESH,
            )
            copy.start()
            sends.append((part, copy))

    def project(name, ref, start):
        loads[name].wait()
        size = ref.shape[1]
        part = dot(scaled, ref[...])
        sbuf[:, :, start : start + size] = part.reshape(nkv, rows, size).astype(BF16)

    project("write", write, 0)
    project("read", read, cw)
    pl.semaphore_wait(barrier, nkv - 1 + ntp - 1)
    exchange(saux, raux, 0, None, 0)
    exchange(sbuf, rbuf, 0, 2 * cw, 1)
    project("value", value, 2 * cw)
    exchange(sbuf, rbuf, 2 * cw, cv, 2)
    project("gate", gate, 2 * cw + cv)
    exchange(sbuf, rbuf, 2 * cw + cv, cv, 3)

    for name in (
        "acc", "rawv", "raww", "rawr", "tapv", "tapw", "tapr", "bias", "rate", "direct",
        "prior", "extra",
    ):
        loads[name].wait()
    early = TAPS - 1
    kinds = early + TAPS

    def shifts(ref, count):
        total = None
        for s in range(seqs):
            shape = (count * rows, raw_len)
            index, r = iota(shape, 0), iota(shape, 1)
            kind = lax.div(index, rows)
            within = lax.rem(index, rows)
            t = lax.rem(within, DRAFT)
            here = lax.div(within, DRAFT) == s
            is_early = (kind < early) & (t + kind < early) & (r == acc[s] + t + kind)
            is_last = (kind >= early) & (r == t + kind - early)
            pick = jnp.where(here & (is_early | is_last), 1.0, 0.0).astype(BF16)
            term = dot(pick, ref[s])
            total = term if total is None else total + term
        return total

    def tap(taps, j):
        return taps[j : j + 1, :].astype(F32)

    def early_of(moved, taps):
        return sum(
            moved[j * rows : (j + 1) * rows] * tap(taps, j) for j in range(early)
        )

    def last_of(moved, taps):
        return silu(
            sum(
                moved[(early + j) * rows : (early + j + 1) * rows] * tap(taps, j)
                for j in range(TAPS)
            )
        )

    moved = shifts(rawv, kinds)
    early_v = early_of(moved, tapv)
    last_v = last_of(moved, tapv)
    moved = shifts(raww, kinds)
    early_w = early_of(moved, tapw)
    last_w = last_of(moved, tapw)
    early_r = early_of(shifts(rawr, early), tapr)

    square = (rows, rows)
    ri, ci = iota(square, 0), iota(square, 1)
    same = lax.div(ri, DRAFT) == lax.div(ci, DRAFT)

    def mix(mask, x):
        return dot(jnp.where(mask, 1.0, 0.0), x, precision=lax.Precision.HIGHEST)

    spread = jnp.where(
        lax.div(iota((heads, cv), 1), HEAD_DIM) == iota((heads, cv), 0), 1.0, 0.0
    ).astype(BF16)

    def expand(x):
        high, low = split(x)
        return dot(high, spread) + dot(low, spread)

    head_shape = (rows, heads)
    row_h = iota(head_shape, 0)
    rate_e = jnp.exp(rate[...])
    seq_h = lax.div(row_h, DRAFT)
    accepted = jnp.zeros(head_shape, jnp.int32)
    for s in range(seqs):
        accepted = jnp.where(seq_h == s, acc[s], accepted)
    live = jnp.where(lax.rem(row_h, DRAFT) < accepted, 1.0, 0.0)
    prior_x = jnp.concatenate([prior[s] for s in range(seqs)], axis=0)
    extra_p = jnp.concatenate([extra[s, :DRAFT] for s in range(seqs)], axis=0)
    extra_n = jnp.concatenate([extra[s, DRAFT:] for s in range(seqs)], axis=0)
    prior_step = softplus(prior_x + bias[...])
    kept = live * (extra_p - rate_e * prior_step)
    total_decay = jnp.exp(mix(same, kept))
    tail = mix(same & (ci > ri), kept)
    coefficient = expand(live * jnp.exp(tail) * prior_step)
    direct_e = expand(jnp.broadcast_to(direct[...], head_shape))
    weighted = coefficient * last_v
    row_c = lax.div(iota((rows, width), 0), DRAFT)
    loads["state"].wait()
    for g in range(groups):
        lanes = slice(g * STATE, (g + 1) * STATE)
        for s in range(seqs):
            a = jnp.where(row_c == s, weighted[:, g * width : (g + 1) * width], 0.0)
            added = dot(a, last_w[:, lanes], ((0,), (0,)), lax.Precision.HIGHEST)
            for i in range(per_group):
                h = g * per_group + i
                decay = total_decay[s * DRAFT : s * DRAFT + 1, h : h + 1]
                new = decay * state[s, h] + added[i * HEAD_DIM : (i + 1) * HEAD_DIM]
                res_ref[s, h] = new
                high, low = split(new)
                at = slice(h * HEAD_DIM, (h + 1) * HEAD_DIM)
                s_hi[s, at] = high
                s_lo[s, at] = low

    def arrive(part):
        for p, copy in sends:
            if p == part:
                copy.wait_recv()

    arrive(0)
    aux = saux[me]
    for off in range(1, nkv):
        aux = aux + raux[off - 1]
    inverse = lax.rsqrt(aux[:, :1] * (1.0 / (depth * nkv)) + EPS)
    step_pre = inverse * aux[:, STATE : STATE + heads]
    step_now = softplus(step_pre + bias[...])
    log_decay = extra_n - rate_e * step_now
    cumulative = mix(same & (ci <= ri), log_decay)
    stack = [jnp.exp(cumulative)]
    for d in range(DRAFT):
        if d == 0:
            stack.append(step_now)
        else:
            back = same & (ci == ri - d)
            gap = cumulative - mix(back, cumulative)
            stack.append(jnp.exp(jnp.minimum(gap, 0.0)) * mix(back, step_now))
    wide = expand(jnp.concatenate(stack, axis=0))
    carry_e = wide[:rows]
    coef = [wide[(d + 1) * rows : (d + 2) * rows] for d in range(DRAFT)]

    def summed(start, size):
        total = sbuf[me, :, start : start + size].astype(F32)
        for off in range(1, nkv):
            total = total + rbuf[off - 1, :, start : start + size].astype(F32)
        return (inverse * total).astype(BF16).astype(F32)

    def delayed(x, d):
        if d == 0:
            return x
        keep = lax.rem(iota(x.shape, 0), DRAFT) >= d
        return jnp.where(keep, pltpu.roll(x, d, 0), 0.0)

    def conv(before, new, taps):
        total = before
        for d in range(DRAFT):
            total = total + tap(taps, TAPS - 1 - d) * delayed(new, d)
        return silu(total)

    arrive(1)
    writes = conv(early_w, summed(0, cw), tapw)
    reads = conv(early_r, summed(cw, cw), tapr)
    r_hi, r_lo = split(reads)
    r_both = jnp.concatenate([r_hi, r_lo], axis=0)
    carried = []
    for g in range(groups):
        lanes = slice(g * STATE, (g + 1) * STATE)
        result = None
        for s in range(seqs):
            at = slice(g * width, (g + 1) * width)
            both = dot(r_both[:, lanes], s_hi[s, at], ((1,), (1,)))
            low = dot(r_hi[:, lanes], s_lo[s, at], ((1,), (1,)))
            one = both[:rows] + both[rows:] + low
            result = one if result is None else jnp.where(row_c == s, one, result)
        carried.append(result)
    inner = []
    for d in range(DRAFT):
        product = reads * delayed(writes, d)
        inner.append(
            [
                jnp.sum(product[:, g * STATE : (g + 1) * STATE], axis=1, keepdims=True)
                for g in range(groups)
            ]
        )

    arrive(2)
    values = conv(early_v, summed(2 * cw, cv), tapv)
    moved_values = [delayed(values, d) for d in range(DRAFT)]
    mixed = []
    for g in range(groups):
        at = slice(g * width, (g + 1) * width)
        one = carry_e[:, at] * carried[g] + direct_e[:, at] * values[:, at]
        for d in range(DRAFT):
            one = one + inner[d][g] * coef[d][:, at] * moved_values[d][:, at]
        mixed.append(one)

    arrive(3)
    loads["gng"].wait()
    opened = silu(summed(2 * cw + cv, cv))
    for g in range(groups):
        at = slice(g * width, (g + 1) * width)
        gated = mixed[g] * opened[:, at]
        scale = lax.rsqrt(
            jnp.sum(gated * gated, axis=1, keepdims=True) * (1.0 / width) + EPS
        )
        gbuf[me, :, at] = (gated * scale * gng[:, at]).astype(BF16)

    gathers = []
    for off in range(1, nkv):
        peer = lax.rem(me + off, nkv)
        copy = pltpu.make_async_remote_copy(
            src_ref=gbuf.at[me], dst_ref=gbuf.at[me],
            send_sem=gsend_sem.at[off - 1], recv_sem=grecv_sem.at[off - 1],
            device_id={"kv": peer}, device_id_type=MESH,
        )
        copy.start()
        gathers.append(copy)
    loads["outm"].wait()
    for copy in gathers:
        copy.wait_recv()
    share = tokens // ntp
    normed = gbuf[...].astype(F32).reshape(tokens, cv).astype(BF16)
    partial = dot(normed, outm[...])
    pbuf[...] = partial.reshape(ntp, share, outm.shape[1]).astype(BF16)
    parts = []
    for off in range(1, ntp):
        peer = lax.rem(my_tp + off, ntp)
        copy = pltpu.make_async_remote_copy(
            src_ref=pbuf.at[peer], dst_ref=qbuf.at[off - 1],
            send_sem=psend_sem.at[off - 1], recv_sem=precv_sem.at[off - 1],
            device_id={"tp": peer}, device_id_type=MESH,
        )
        copy.start()
        parts.append(copy)
    total = pbuf[my_tp].astype(F32)
    for off in range(1, ntp):
        parts[off - 1].wait_recv()
        total = total + qbuf[off - 1].astype(F32)
    out_ref[...] = total.astype(BF16)
    for _, copy in sends:
        copy.wait_send()
    for copy in gathers + parts:
        copy.wait_send()


def per_device(nkv, ntp, *args):
    flat = [x.reshape(1, -1) if x.ndim == 1 and x.dtype == F32 else x for x in args]
    tokens = args[0].shape[0]
    rows = tokens // nkv
    gate, value, write, read, step = args[2:7]
    outm = args[21]
    cv, cw = value.shape[1], write.shape[1]
    total = gate.shape[1] + cv + 2 * cw
    state = args[19]
    scratch = []
    for i, x in enumerate(flat):
        space = pltpu.SMEM if i == 18 else pltpu.VMEM
        scratch.append(space(x.shape, x.dtype))
    DMA = pltpu.SemaphoreType.DMA
    scratch += [
        pltpu.VMEM((nkv, rows, total), BF16),
        pltpu.VMEM((nkv - 1, rows, total), BF16),
        pltpu.VMEM((nkv, rows, 2 * STATE), F32),
        pltpu.VMEM((nkv - 1, rows, 2 * STATE), F32),
        pltpu.VMEM((nkv, rows, cv), BF16),
        pltpu.VMEM((ntp, tokens // ntp, outm.shape[1]), BF16),
        pltpu.VMEM((ntp - 1, tokens // ntp, outm.shape[1]), BF16),
        pltpu.VMEM((state.shape[0], cv, STATE), BF16),
        pltpu.VMEM((state.shape[0], cv, STATE), BF16),
        DMA((len(flat),)),
        DMA((4, nkv - 1)),
        DMA((4, nkv - 1)),
        DMA((nkv - 1,)),
        DMA((nkv - 1,)),
        DMA((ntp - 1,)),
        DMA((ntp - 1,)),
    ]
    return pl.pallas_call(
        functools.partial(body, nkv, ntp),
        out_shape=(
            jax.ShapeDtypeStruct((tokens // ntp, outm.shape[1]), BF16),
            jax.ShapeDtypeStruct(state.shape, F32),
        ),
        in_specs=[pl.BlockSpec(memory_space=pl.ANY)] * len(flat),
        out_specs=(
            pl.BlockSpec(memory_space=pltpu.VMEM),
            pl.BlockSpec(memory_space=pltpu.VMEM),
        ),
        scratch_shapes=scratch,
        compiler_params=pltpu.CompilerParams(collective_id=0, has_side_effects=True),
        name="mixer",
    )(*flat)


def solution(mesh):
    placed = (
        P(None, "kv"),
        P("kv"),
        P("kv", "tp"),
        P("kv", "tp"),
        P("kv", "tp"),
        P("kv", "tp"),
        P("kv", "tp"),
        P("kv", None, "tp"),
        P("kv", None, "tp"),
        P("kv", None, "tp"),
        P(None, "tp"),
        P(None, "tp"),
        P(None, "tp"),
        P("tp"),
        P("tp"),
        P("tp"),
        P("kv", None, "tp"),
        P("kv", None, "tp"),
        P("kv"),
        P("kv", "tp", None, None),
        P("tp"),
        P("tp", "kv"),
    )
    return jax.shard_map(
        functools.partial(per_device, mesh.shape["kv"], mesh.shape["tp"]),
        mesh=mesh,
        in_specs=placed,
        out_specs=(P("tp", "kv"), P("kv", "tp", None, None)),
        check_vma=False,
    )
```

time: 142 us -> 35.3 us (0.25)
  blocking collectives: 69.9 us -> 0 us
  waiting for transfers between devices: 42.3 us -> 0 us
  Pallas kernels: 0 us -> 27.3 us
  between operations: 15.1 us -> 0.66 us
  matrix products: 8.08 us -> 0 us
  local copies, waits for them, and re-layouts: 3.45 us -> 6.97 us
  other arithmetic: 2.55 us -> 0 us
    reduce_scatter x2 -> x0, waiting for transfers between devices: 42.2 us -> none  [the longest x1 23.7 us: per_device(): lax.psum_scatter(main_part, 'kv', scatter_dimension=0, tiled=True)]
    unnamed x1 -> x0, blocking collectives: 39.3 us -> none
    all_gather x1 -> x0, blocking collectives: 30.5 us -> none  [per_device(): lax.all_gather(normalized_hidden, 'kv', axis=0, tiled=True)]
    pallas_call x0 -> x1, Pallas kernels: none -> 27.3 us  [per_device(): pl.pallas_call(functools.partial(body, nkv, ntp), out_shape=(jax.ShapeDty...]
    dot_general x7 -> x0, matrix products: 8.08 us -> none  [the longest x1 2.71 us: per_device(): main_part = jnp.dot(scaled, joined, preferred_element_type=jnp.float32)]
    unnamed x41 -> x12, local copies, waits for them, and re-layouts: 0.69 us -> 6.97 us
    gather x7 -> x0, local copies, waits for them, and re-layouts: 2 us -> none  [current(): earlier = jnp.take_along_axis(row_block, window[:, :, None], axis=1)]
  transfers between devices with their start and end apart: 2 -> 0, of which waited for: 2 -> 0; matrix products, arithmetic and copies ran while one was open for 3% -> 0% of each run, Pallas kernels for 0% -> 0%
where the time goes in v1:
time: 35.3 us; the launch traced here: 34.9 us
  Pallas kernels  27.3 us (77%)
  local copies, waits for them, and re-layouts  6.97 us (20%)
  between operations  0.66 us (2%)
    pallas_call x1, Pallas kernels, per_device(): pl.pallas_call(functools.partial(body, nkv, ntp), out_shape=(jax.ShapeDty...  27.3 us
    unnamed x12, local copies, waits for them, and re-layouts  6.97 us

profile of v1, /device:TPU:0, one launch (start us, length us, event | category | flops | bytes accessed | tf_op | source)
XLA Modules:
  0.0 34.9 jit_solution(912530617478305984)
XLA Ops:
  0.6 0.0 copy-start.1
  0.6 0.0 copy-start
  0.7 1.3 %copy.26.refs_8_ = bf16[2,7,512]{2,1,0:T(8,128)(2,1)} copy(bf16[2,7,512]{2,0,1:T(2,128)(2,1)} %param.30) | data formatting | bytes 28672 | tf_op args[8]
  2.0 0.0 copy-done.1
  2.0 0.6 %copy.27.refs_9_ = bf16[2,7,512]{2,1,0:T(8,128)(2,1)} copy(bf16[2,7,512]{2,0,1:T(2,128)(2,1)S(1)} %copy-done.1) | data formatting | bytes 28672 | tf_op args[9]
  2.6 0.0 copy-done
  2.6 0.0 copy-start.2
  2.6 0.6 %copy.25.refs_7_ = bf16[2,7,1024]{2,1,0:T(8,128)(2,1)} copy(bf16[2,7,1024]{2,0,1:T(2,128)(2,1)S(1)} %copy-done) | data formatting | bytes 57344 | tf_op args[7]
  3.2 0.1 copy-done.2
  3.3 0.7 %copy.24.refs_6_ = bf16[256,16]{1,0:T(8,128)(2,1)} copy(bf16[256,16]{0,1:T(8,128)(2,1)S(1)} %copy-done.2) | data formatting | bytes 16384 | tf_op args[6]
  4.0 27.3 %mixer.1 = (bf16[16,256]{1,0:T(8,128)(2,1)}, f32[2,16,64,128]{3,2,1,0:T(8,128)}) custom-call(bf16[64,256]{1,0:T(8,128)(2,1)} %refs_0_.1, f32[1,256]{1,0:T(1,128)} %bitcast.6, bf16[256,1024]{1,0:T(8,128)(2,1)} %refs_2_.1, bf16[256,1024]{1,0:T(8,128)(2,1)} %refs_3_.1, bf16[256,512]{1,0:T(8,128)(2,1)} %refs_4_.1, bf16[256,512]{1,0:T(8,128)(2,1)} %refs_5_.1, ...), custom_call_target="tpu_custom_call" | custom-call | tf_op jit(solution)/shard_map/mixer/pallas_call | solution.py:395
  31.3 1.3 %copy.30 = bf16[16,256]{1,0:T(8,128)(2,1)} copy(bf16[16,256]{1,0:T(8,128)(2,1)} %get-tuple-element.4) | data formatting | bytes 16384
  32.6 2.3 %copy.31 = f32[2,16,64,128]{3,2,1,0:T(8,128)} copy(f32[2,16,64,128]{3,2,1,0:T(8,128)} %get-tuple-element.5) | data formatting | bytes 2097152
Async XLA Ops:
  0.6 1.4 %copy-start.1 = (bf16[2,7,512]{2,0,1:T(2,128)(2,1)S(1)}, bf16[2,7,512]{2,0,1:T(2,128)(2,1)}, u32[]{:S(2)}) copy-start(bf16[2,7,512]{2,0,1:T(2,128)(2,1)} %param.31) | copy-start | bytes 43012
  0.6 2.0 %copy-start = (bf16[2,7,1024]{2,0,1:T(2,128)(2,1)S(1)}, bf16[2,7,1024]{2,0,1:T(2,128)(2,1)}, u32[]{:S(2)}) copy-start(bf16[2,7,1024]{2,0,1:T(2,128)(2,1)} %param.29) | copy-start | bytes 86020
  2.6 0.7 %copy-start.2 = (bf16[256,16]{0,1:T(8,128)(2,1)S(1)}, bf16[256,16]{0,1:T(8,128)(2,1)}, u32[]{:S(2)}) copy-start(bf16[256,16]{0,1:T(8,128)(2,1)} %param.28) | copy-start | bytes 24580

commit v2 on v1

--- a/solution.py
+++ b/solution.py
@@ -47,20 +47,26 @@
         out_ref, res_ref,
         hid, gain, gate, value, write, read, step, rawv, raww, rawr,
         tapv, tapw, tapr, bias, rate, direct, prior, extra, acc, state, gng, outm,
-        sbuf, rbuf, saux, raux, gbuf, pbuf, qbuf, s_hi, s_lo,
-        load_sem, send_sem, recv_sem, gsend_sem, grecv_sem, psend_sem, precv_sem,
+        sbuf, fbuf, nbuf, xs, xr, saux, faux, naux, xsa, xra,
+        gbuf, pbuf, qbuf, s_hi, s_lo,
+        load_sem, f_send, f_recv, n_send, n_recv, x_send, x_recv,
+        gsend_sem, grecv_sem, psend_sem, precv_sem,
     ) = refs
     me = lax.axis_index("kv")
     my_tp = lax.axis_index("tp")
-    rows = sbuf.shape[1]
-    seqs = rawv.shape[0]
+    chunks, _, rows, _ = sbuf.shape
+    inner = nkv // 2
+    place = lax.rem(me, inner)
+    mine = me - place
+    theirs = inner - mine
+    seqs = rawv.shape[1]
     tokens, depth = hid.shape
-    heads = step.shape[1]
+    heads = step.shape[0]
     cv, cw = value.shape[1], write.shape[1]
     groups = cw // STATE
     width = cv // groups
     per_group = heads // groups
-    raw_len = rawv.shape[1]
+    raw_len = rawv.shape[0]
     MESH = pl.DeviceIdType.MESH
 
     loads = {}
@@ -94,43 +100,75 @@
     floats = hid[...].astype(F32)
     squares = jnp.sum(floats * floats, axis=1, keepdims=True)
     scaled = (floats * gain[...]).astype(BF16)
-    saux[:, :, :STATE] = jnp.broadcast_to(squares, (tokens, STATE)).reshape(nkv, rows, STATE)
-    saux[:, :, STATE:] = jnp.zeros((nkv, rows, STATE), F32)
-    saux[:, :, STATE : STATE + heads] = dot(scaled, step[...]).reshape(nkv, rows, heads)
-
-    sends = []
-
-    def exchange(buffer, target, start, size, part):
-        for off in range(1, nkv):
-            peer = lax.rem(me + off, nkv)
-            if size is None:
-                src, dst = buffer.at[peer], target.at[off - 1]
-            else:
-                src = buffer.at[peer, :, pl.ds(start, size)]
-                dst = target.at[off - 1, :, pl.ds(start, size)]
+    saux[...] = jnp.broadcast_to(squares, (tokens, STATE)).reshape(nkv, rows, STATE)
+    saux[:, :, :heads] = dot(scaled, step[...], ((1,), (1,))).reshape(nkv, rows, heads)
+    wc, vc, gc = cw // chunks, cv // chunks, groups // chunks
+
+    def project(name, ref, start):
+        loads[name].wait()
+        size = ref.shape[1] // chunks
+        part = dot(scaled, ref[...])
+        for c in range(chunks):
+            piece = part[:, c * size : (c + 1) * size].reshape(nkv, rows, size)
+            sbuf[c, :, :, start : start + size] = piece.astype(BF16)
+
+    project("write", write, 0)
+    project("read", read, wc)
+    project("value", value, 2 * wc)
+    project("gate", gate, 2 * wc + vc)
+
+    def source(part, half, rank):
+        if part == chunks:
+            return saux.at[half + rank]
+        return sbuf.at[part, half + rank]
+
+    def spread_out(part, half, target, target_aux, send, recv):
+        copies = []
+        for off in range(1, inner):
+            rank = lax.rem(place + off, inner)
+            dst = target_aux.at[off - 1] if part == chunks else target.at[part, off - 1]
             copy = pltpu.make_async_remote_copy(
-                src_ref=src, dst_ref=dst,
-                send_sem=send_sem.at[part, off - 1], recv_sem=recv_sem.at[part, off - 1],
-                device_id={"kv": peer}, device_id_type=MESH,
+                src_ref=source(part, half, rank), dst_ref=dst,
+                send_sem=send.at[part, off - 1], recv_sem=recv.at[part, off - 1],
+                device_id={"kv": mine + rank}, device_id_type=MESH,
             )
             copy.start()
-            sends.append((part, copy))
-
-    def project(name, ref, start):
-        loads[name].wait()
-        size = ref.shape[1]
-        part = dot(scaled, ref[...])
-        sbuf[:, :, start : start + size] = part.reshape(nkv, rows, size).astype(BF16)
-
-    project("write", write, 0)
-    project("read", read, cw)
+            copies.append(copy)
+        return copies
+
     pl.semaphore_wait(barrier, nkv - 1 + ntp - 1)
-    exchange(saux, raux, 0, None, 0)
-    exchange(sbuf, rbuf, 0, 2 * cw, 1)
-    project("value", value, 2 * cw)
-    exchange(sbuf, rbuf, 2 * cw, cv, 2)
-    project("gate", gate, 2 * cw + cv)
-    exchange(sbuf, rbuf, 2 * cw + cv, cv, 3)
+    parts_order = (chunks,) + tuple(range(chunks))
+    far = {p: spread_out(p, theirs, fbuf, faux, f_send, f_recv) for p in parts_order}
+    near = {p: spread_out(p, mine, nbuf, naux, n_send, n_recv) for p in parts_order}
+    cross = {}
+
+    def forward(part):
+        for copy in far[part]:
+            copy.wait_recv()
+        if part == chunks:
+            total = saux[theirs + place]
+            for off in range(1, inner):
+                total = total + faux[off - 1]
+            xsa[...] = total
+            src, dst = xsa, xra
+        else:
+            total = sbuf[part, theirs + place].astype(F32)
+            for off in range(1, inner):
+                total = total + fbuf[part, off - 1].astype(F32)
+            xs[part] = total.astype(BF16)
+            src, dst = xs.at[part], xr.at[part]
+        copy = pltpu.make_async_remote_copy(
+            src_ref=src, dst_ref=dst,
+            send_sem=x_send.at[part], recv_sem=x_recv.at[part],
+            device_id={"kv": theirs + place}, device_id_type=MESH,
+        )
+        copy.start()
+        cross[part] = copy
+
+    def arrive(part):
+        for copy in near[part]:
+            copy.wait_recv()
+        cross[part].wait_recv()
 
     for name in (
         "acc", "rawv", "raww", "rawr", "tapv", "tapw", "tapr", "bias", "rate", "direct",
@@ -141,20 +179,22 @@
     kinds = early + TAPS
 
     def shifts(ref, count):
-        total = None
+        flat = jnp.concatenate([ref[r].astype(F32) for r in range(raw_len)], axis=0)
+        shape = (count * rows, raw_len * seqs)
+        index, column = iota(shape, 0), iota(shape, 1)
+        kind = lax.div(index, rows)
+        within = lax.rem(index, rows)
+        t = lax.rem(within, DRAFT)
+        seq = lax.div(within, DRAFT)
+        r = lax.div(column, seqs)
+        begin = jnp.zeros(shape, jnp.int32)
         for s in range(seqs):
-            shape = (count * rows, raw_len)
-            index, r = iota(shape, 0), iota(shape, 1)
-            kind = lax.div(index, rows)
-            within = lax.rem(index, rows)
-            t = lax.rem(within, DRAFT)
-            here = lax.div(within, DRAFT) == s
-            is_early = (kind < early) & (t + kind < early) & (r == acc[s] + t + kind)
-            is_last = (kind >= early) & (r == t + kind - early)
-            pick = jnp.where(here & (is_early | is_last), 1.0, 0.0).astype(BF16)
-            term = dot(pick, ref[s])
-            total = term if total is None else total + term
-        return total
+            begin = jnp.where(seq == s, acc[s], begin)
+        is_early = (kind < early) & (t + kind < early) & (r == begin + t + kind)
+        is_last = (kind >= early) & (r == t + kind - early)
+        here = seq == lax.rem(column, seqs)
+        pick = jnp.where(here & (is_early | is_last), 1.0, 0.0).astype(BF16)
+        return dot(pick, flat.astype(BF16))
 
     def tap(taps, j):
         return taps[j : j + 1, :].astype(F32)
@@ -214,6 +254,8 @@
     direct_e = expand(jnp.broadcast_to(direct[...], head_shape))
     weighted = coefficient * last_v
     row_c = lax.div(iota((rows, width), 0), DRAFT)
+    for part in parts_order:
+        forward(part)
     loads["state"].wait()
     for g in range(groups):
         lanes = slice(g * STATE, (g + 1) * STATE)
@@ -230,17 +272,12 @@
                 s_hi[s, at] = high
                 s_lo[s, at] = low
 
-    def arrive(part):
-        for p, copy in sends:
-            if p == part:
-                copy.wait_recv()
-
-    arrive(0)
-    aux = saux[me]
-    for off in range(1, nkv):
-        aux = aux + raux[off - 1]
-    inverse = lax.rsqrt(aux[:, :1] * (1.0 / (depth * nkv)) + EPS)
-    step_pre = inverse * aux[:, STATE : STATE + heads]
+    arrive(chunks)
+    aux = saux[me] + xra[...]
+    for off in range(1, inner):
+        aux = aux + naux[off - 1]
+    inverse = lax.rsqrt(aux[:, STATE - 1 :] * (1.0 / (depth * nkv)) + EPS)
+    step_pre = inverse * aux[:, :heads]
     step_now = softplus(step_pre + bias[...])
     log_decay = extra_n - rate_e * step_now
     cumulative = mix(same & (ci <= ri), log_decay)
@@ -256,10 +293,11 @@
     carry_e = wide[:rows]
     coef = [wide[(d + 1) * rows : (d + 2) * rows] for d in range(DRAFT)]
 
-    def summed(start, size):
-        total = sbuf[me, :, start : start + size].astype(F32)
-        for off in range(1, nkv):
-            total = total + rbuf[off - 1, :, start : start + size].astype(F32)
+    def summed(part, start, size):
+        at = slice(start, start + size)
+        total = sbuf[part, me, :, at].astype(F32) + xr[part, :, at].astype(F32)
+        for off in range(1, inner):
+            total = total + nbuf[part, off - 1, :, at].astype(F32)
         return (inverse * total).astype(BF16).astype(F32)
 
     def delayed(x, d):
@@ -268,76 +306,67 @@
         keep = lax.rem(iota(x.shape, 0), DRAFT) >= d
         return jnp.where(keep, pltpu.roll(x, d, 0), 0.0)
 
-    def conv(before, new, taps):
-        total = before
+    def conv(before, new, taps, begin):
+        at = slice(begin, begin + new.shape[1])
+        total = before[:, at]
         for d in range(DRAFT):
-            total = total + tap(taps, TAPS - 1 - d) * delayed(new, d)
+            total = total + tap(taps, TAPS - 1 - d)[:, at] * delayed(new, d)
         return silu(total)
 
-    arrive(1)
-    writes = conv(early_w, summed(0, cw), tapw)
-    reads = conv(early_r, summed(cw, cw), tapr)
-    r_hi, r_lo = split(reads)
-    r_both = jnp.concatenate([r_hi, r_lo], axis=0)
-    carried = []
-    for g in range(groups):
-        lanes = slice(g * STATE, (g + 1) * STATE)
-        result = None
-        for s in range(seqs):
+    loads["gng"].wait()
+    gathers = []
+    for c in range(chunks):
+        arrive(c)
+        writes = conv(early_w, summed(c, 0, wc), tapw, c * wc)
+        reads = conv(early_r, summed(c, wc, wc), tapr, c * wc)
+        values = conv(early_v, summed(c, 2 * wc, vc), tapv, c * vc)
+        opened = silu(summed(c, 2 * wc + vc, vc))
+        r_hi, r_lo = split(reads)
+        r_both = jnp.concatenate([r_hi, r_lo], axis=0)
+        moved_writes = [delayed(writes, d) for d in range(DRAFT)]
+        moved_values = [delayed(values, d) for d in range(DRAFT)]
+        for k in range(gc):
+            g = c * gc + k
+            lanes = slice(k * STATE, (k + 1) * STATE)
+            near_at = slice(k * width, (k + 1) * width)
             at = slice(g * width, (g + 1) * width)
-            both = dot(r_both[:, lanes], s_hi[s, at], ((1,), (1,)))
-            low = dot(r_hi[:, lanes], s_lo[s, at], ((1,), (1,)))
-            one = both[:rows] + both[rows:] + low
-            result = one if result is None else jnp.where(row_c == s, one, result)
-        carried.append(result)
-    inner = []
-    for d in range(DRAFT):
-        product = reads * delayed(writes, d)
-        inner.append(
-            [
-                jnp.sum(product[:, g * STATE : (g + 1) * STATE], axis=1, keepdims=True)
-                for g in range(groups)
-            ]
-        )
-
-    arrive(2)
-    values = conv(early_v, summed(2 * cw, cv), tapv)
-    moved_values = [delayed(values, d) for d in range(DRAFT)]
-    mixed = []
-    for g in range(groups):
-        at = slice(g * width, (g + 1) * width)
-        one = carry_e[:, at] * carried[g] + direct_e[:, at] * values[:, at]
-        for d in range(DRAFT):
-            one = one + inner[d][g] * coef[d][:, at] * moved_values[d][:, at]
-        mixed.append(one)
-
-    arrive(3)
-    loads["gng"].wait()
-    opened = silu(summed(2 * cw + cv, cv))
-    for g in range(groups):
-        at = slice(g * width, (g + 1) * width)
-        gated = mixed[g] * opened[:, at]
-        scale = lax.rsqrt(
-            jnp.sum(gated * gated, axis=1, keepdims=True) * (1.0 / width) + EPS
-        )
-        gbuf[me, :, at] = (gated * scale * gng[:, at]).astype(BF16)
-
-    gathers = []
-    for off in range(1, nkv):
-        peer = lax.rem(me + off, nkv)
-        copy = pltpu.make_async_remote_copy(
-            src_ref=gbuf.at[me], dst_ref=gbuf.at[me],
-            send_sem=gsend_sem.at[off - 1], recv_sem=grecv_sem.at[off - 1],
-            device_id={"kv": peer}, device_id_type=MESH,
-        )
-        copy.start()
-        gathers.append(copy)
+            carried = None
+            for s in range(seqs):
+                both = dot(r_both[:, lanes], s_hi[s, at], ((1,), (1,)))
+                low = dot(r_hi[:, lanes], s_lo[s, at], ((1,), (1,)))
+                one = both[:rows] + both[rows:] + low
+                carried = one if carried is None else jnp.where(row_c == s, one, carried)
+            mixed = carry_e[:, at] * carried + direct_e[:, at] * values[:, near_at]
+            for d in range(DRAFT):
+                product = jnp.sum(
+                    reads[:, lanes] * moved_writes[d][:, lanes], axis=1, keepdims=True
+                )
+                mixed = mixed + product * coef[d][:, at] * moved_values[d][:, near_at]
+            gated = mixed * opened[:, near_at]
+            scale = lax.rsqrt(
+                jnp.sum(gated * gated, axis=1, keepdims=True) * (1.0 / width) + EPS
+            )
+            gbuf[c, me, :, near_at] = (gated * scale * gng[:, at]).astype(BF16)
+
+        for off in range(nkv - 1, 0, -1):
+            peer = lax.rem(me + off, nkv)
+            copy = pltpu.make_async_remote_copy(
+                src_ref=gbuf.at[c, me], dst_ref=gbuf.at[c, me],
+                send_sem=gsend_sem.at[c, off - 1], recv_sem=grecv_sem.at[c, off - 1],
+                device_id={"kv": peer}, device_id_type=MESH,
+            )
+            copy.start()
+            gathers.append((c, copy))
     loads["outm"].wait()
-    for copy in gathers:
-        copy.wait_recv()
     share = tokens // ntp
-    normed = gbuf[...].astype(F32).reshape(tokens, cv).astype(BF16)
-    partial = dot(normed, outm[...])
+    partial = None
+    for c in range(chunks):
+        for k, copy in gathers:
+            if k == c:
+                copy.wait_recv()
+        normed = gbuf[c].astype(F32).reshape(tokens, vc).astype(BF16)
+        term = dot(normed, outm[c * vc : (c + 1) * vc])
+        partial = term if partial is None else partial + term
     pbuf[...] = partial.reshape(ntp, share, outm.shape[1]).astype(BF16)
     parts = []
     for off in range(1, ntp):
@@ -354,20 +383,27 @@
         parts[off - 1].wait_recv()
         total = total + qbuf[off - 1].astype(F32)
     out_ref[...] = total.astype(BF16)
-    for _, copy in sends:
-        copy.wait_send()
-    for copy in gathers + parts:
+    for p in parts_order:
+        for copy in far[p] + near[p] + [cross[p]]:
+            copy.wait_send()
+    for copy in [copy for _, copy in gathers] + parts:
         copy.wait_send()
 
 
 def per_device(nkv, ntp, *args):
     flat = [x.reshape(1, -1) if x.ndim == 1 and x.dtype == F32 else x for x in args]
+    flat[6] = flat[6].T
+    for i in (7, 8, 9):
+        flat[i] = flat[i].transpose(1, 0, 2)
     tokens = args[0].shape[0]
     rows = tokens // nkv
     gate, value, write, read, step = args[2:7]
     outm = args[21]
     cv, cw = value.shape[1], write.shape[1]
-    total = gate.shape[1] + cv + 2 * cw
+    groups = cw // STATE
+    chunks = 2 if groups % 2 == 0 else 1
+    inner = nkv // 2
+    total = (gate.shape[1] + cv + 2 * cw) // chunks
     state = args[19]
     scratch = []
     for i, x in enumerate(flat):
@@ -375,28 +411,38 @@
         scratch.append(space(x.shape, x.dtype))
     DMA = pltpu.SemaphoreType.DMA
     scratch += [
-        pltpu.VMEM((nkv, rows, total), BF16),
-        pltpu.VMEM((nkv - 1, rows, total), BF16),
-        pltpu.VMEM((nkv, rows, 2 * STATE), F32),
-        pltpu.VMEM((nkv - 1, rows, 2 * STATE), F32),
-        pltpu.VMEM((nkv, rows, cv), BF16),
+        pltpu.VMEM((chunks, nkv, rows, total), BF16),
+        pltpu.VMEM((chunks, inner - 1, rows, total), BF16),
+        pltpu.VMEM((chunks, inner - 1, rows, total), BF16),
+        pltpu.VMEM((chunks, rows, total), BF16),
+        pltpu.VMEM((chunks, rows, total), BF16),
+        pltpu.VMEM((nkv, rows, STATE), F32),
+        pltpu.VMEM((inner - 1, rows, STATE), F32),
+        pltpu.VMEM((inner - 1, rows, STATE), F32),
+        pltpu.VMEM((rows, STATE), F32),
+        pltpu.VMEM((rows, STATE), F32),
+        pltpu.VMEM((chunks, nkv, rows, cv // chunks), BF16),
         pltpu.VMEM((ntp, tokens // ntp, outm.shape[1]), BF16),
         pltpu.VMEM((ntp - 1, tokens // ntp, outm.shape[1]), BF16),
         pltpu.VMEM((state.shape[0], cv, STATE), BF16),
         pltpu.VMEM((state.shape[0], cv, STATE), BF16),
         DMA((len(flat),)),
-        DMA((4, nkv - 1)),
-        DMA((4, nkv - 1)),
-        DMA((nkv - 1,)),
-        DMA((nkv - 1,)),
+        DMA((chunks + 1, inner - 1)),
+        DMA((chunks + 1, inner - 1)),
+        DMA((chunks + 1, inner - 1)),
+        DMA((chunks + 1, inner - 1)),
+        DMA((chunks + 1,)),
+        DMA((chunks + 1,)),
+        DMA((chunks, nkv - 1)),
+        DMA((chunks, nkv - 1)),
         DMA((ntp - 1,)),
         DMA((ntp - 1,)),
     ]
     return pl.pallas_call(
         functools.partial(body, nkv, ntp),
         out_shape=(
-            jax.ShapeDtypeStruct((tokens // ntp, outm.shape[1]), BF16),
-            jax.ShapeDtypeStruct(state.shape, F32),
+            pltpu.VMEM((tokens // ntp, outm.shape[1]), BF16),
+            pltpu.VMEM(state.shape, F32),
         ),
         in_specs=[pl.BlockSpec(memory_space=pl.ANY)] * len(flat),
         out_specs=(

time: 35.3 us -> 26.8 us (0.76)
  local copies, waits for them, and re-layouts: 6.97 us -> 1.57 us
  Pallas kernels: 27.3 us -> 24.4 us
    unnamed x12 -> x2, local copies, waits for them, and re-layouts: 6.97 us -> 1.57 us
    pallas_call x1, Pallas kernels: 27.3 us -> 24.4 us  [per_device(): pl.pallas_call(functools.partial(body, nkv, ntp), out_shape=(pltpu.VMEM((...]
where the time goes in v2:
time: 26.8 us; the launch traced here: 26.7 us
  Pallas kernels  24.4 us (91%)
  local copies, waits for them, and re-layouts  1.57 us (6%)
  between operations  0.65 us (2%)
    pallas_call x1, Pallas kernels, per_device(): pl.pallas_call(functools.partial(body, nkv, ntp), out_shape=(pltpu.VMEM((...  24.4 us
    unnamed x2, local copies, waits for them, and re-layouts  1.57 us

profile of v2, /device:TPU:0, one launch (start us, length us, event | category | flops | bytes accessed | tf_op | source)
XLA Modules:
  0.0 26.7 jit_solution(14964836737223775026)
XLA Ops:
  0.6 24.4 %mixer.1 = (bf16[16,256]{1,0:T(8,128)(2,1)S(1)}, f32[2,16,64,128]{3,2,1,0:T(8,128)S(1)}) custom-call(bf16[64,256]{1,0:T(8,128)(2,1)} %refs_0_.1, f32[1,256]{1,0:T(1,128)} %bitcast.14, bf16[256,1024]{1,0:T(8,128)(2,1)} %refs_2_.1, bf16[256,1024]{1,0:T(8,128)(2,1)} %refs_3_.1, bf16[256,512]{1,0:T(8,128)(2,1)} %refs_4_.1, bf16[256,512]{1,0:T(8,128)(2,1)} %refs_5_.1, ...), custom_call_target="tpu_custom_call" | custom-call | tf_op jit(solution)/shard_map/mixer/pallas_call | solution.py:441
  25.1 0.6 %copy.26 = bf16[16,256]{1,0:T(8,128)(2,1)} copy(bf16[16,256]{1,0:T(8,128)(2,1)S(1)} %get-tuple-element.2) | data formatting | bytes 16384
  25.7 1.0 %copy.27 = f32[2,16,64,128]{3,2,1,0:T(8,128)} copy(f32[2,16,64,128]{3,2,1,0:T(8,128)S(1)} %get-tuple-element.3) | data formatting | bytes 2097152

commit v3 on v2

--- a/solution.py
+++ b/solution.py
@@ -136,11 +136,9 @@
             copies.append(copy)
         return copies
 
-    pl.semaphore_wait(barrier, nkv - 1 + ntp - 1)
     parts_order = (chunks,) + tuple(range(chunks))
-    far = {p: spread_out(p, theirs, fbuf, faux, f_send, f_recv) for p in parts_order}
-    near = {p: spread_out(p, mine, nbuf, naux, n_send, n_recv) for p in parts_order}
     cross = {}
+    far, near = {}, {}
 
     def forward(part):
         for copy in far[part]:
@@ -254,8 +252,6 @@
     direct_e = expand(jnp.broadcast_to(direct[...], head_shape))
     weighted = coefficient * last_v
     row_c = lax.div(iota((rows, width), 0), DRAFT)
-    for part in parts_order:
-        forward(part)
     loads["state"].wait()
     for g in range(groups):
         lanes = slice(g * STATE, (g + 1) * STATE)
@@ -272,6 +268,11 @@
                 s_hi[s, at] = high
                 s_lo[s, at] = low
 
+    pl.semaphore_wait(barrier, nkv - 1 + ntp - 1)
+    far.update({p: spread_out(p, theirs, fbuf, faux, f_send, f_recv) for p in parts_order})
+    near.update({p: spread_out(p, mine, nbuf, naux, n_send, n_recv) for p in parts_order})
+    for part in parts_order:
+        forward(part)
     arrive(chunks)
     aux = saux[me] + xra[...]
     for off in range(1, inner):
@@ -348,8 +349,9 @@
             )
             gbuf[c, me, :, near_at] = (gated * scale * gng[:, at]).astype(BF16)
 
-        for off in range(nkv - 1, 0, -1):
-            peer = lax.rem(me + off, nkv)
+        for off in list(range(inner, nkv)) + list(range(1, inner)):
+            half = theirs if off >= inner else mine
+            peer = half + lax.rem(place + off, inner)
             copy = pltpu.make_async_remote_copy(
                 src_ref=gbuf.at[c, me], dst_ref=gbuf.at[c, me],
                 send_sem=gsend_sem.at[c, off - 1], recv_sem=grecv_sem.at[c, off - 1],

time: 26.8 us -> 26.2 us (0.978)
  Pallas kernels: 24.4 us -> 23.8 us
    pallas_call x1, Pallas kernels: 24.4 us -> 23.8 us  [per_device(): pl.pallas_call(functools.partial(body, nkv, ntp), out_shape=(pltpu.VMEM((...]
where the time goes in v3:
time: 26.2 us; the launch traced here: 26 us
  Pallas kernels  23.8 us (91%)
  local copies, waits for them, and re-layouts  1.57 us (6%)
  between operations  0.65 us (2%)
    pallas_call x1, Pallas kernels, per_device(): pl.pallas_call(functools.partial(body, nkv, ntp), out_shape=(pltpu.VMEM((...  23.8 us
    unnamed x2, local copies, waits for them, and re-layouts  1.57 us

profile of v3, /device:TPU:0, one launch (start us, length us, event | category | flops | bytes accessed | tf_op | source)
XLA Modules:
  0.0 26.0 jit_solution(13386929224799531283)
XLA Ops:
  0.6 23.8 %mixer.1 = (bf16[16,256]{1,0:T(8,128)(2,1)S(1)}, f32[2,16,64,128]{3,2,1,0:T(8,128)S(1)}) custom-call(bf16[64,256]{1,0:T(8,128)(2,1)} %refs_0_.1, f32[1,256]{1,0:T(1,128)} %bitcast.14, bf16[256,1024]{1,0:T(8,128)(2,1)} %refs_2_.1, bf16[256,1024]{1,0:T(8,128)(2,1)} %refs_3_.1, bf16[256,512]{1,0:T(8,128)(2,1)} %refs_4_.1, bf16[256,512]{1,0:T(8,128)(2,1)} %refs_5_.1, ...), custom_call_target="tpu_custom_call" | custom-call | tf_op jit(solution)/shard_map/mixer/pallas_call | solution.py:443
  24.5 0.6 %copy.26 = bf16[16,256]{1,0:T(8,128)(2,1)} copy(bf16[16,256]{1,0:T(8,128)(2,1)S(1)} %get-tuple-element.2) | data formatting | bytes 16384
  25.1 1.0 %copy.27 = f32[2,16,64,128]{3,2,1,0:T(8,128)} copy(f32[2,16,64,128]{3,2,1,0:T(8,128)S(1)} %get-tuple-element.3) | data formatting | bytes 2097152
